TPU v7x, 512 devices: a whole 4x4x16 slice. The times are simulated.
512 devices in a mesh: sp: 32 (over z, core), tp: 16 (over y, x).
Axes of the slice: x: 4, y: 4, z: 16, core: 2. Of those that a mesh axis runs over, the one named last changes fastest.
Arguments:
- query_a: bfloat16 [1024, 4096], P('tp', 'sp'), may hold values from -16 to 16
- key_a: bfloat16 [1024, 4096], P('tp', 'sp'), may hold values from -6 to 6
- value_a: bfloat16 [1024, 4096], P('tp', 'sp'), may hold values from -6 to 6
- cumlog_a: float32 [16, 4096], P('tp'), as said below
- query_b: bfloat16 [2048, 4096], P('tp', 'sp'), may hold values from -16 to 16
- key_b: bfloat16 [2048, 4096], P('tp', 'sp'), may hold values from -6 to 6
- value_b: bfloat16 [2048, 4096], P('tp', 'sp'), may hold values from -6 to 6
- cumlog_b: float32 [16, 4096], P('tp'), as said below
- out_weight_a: bfloat16 [1024, 2048], P('tp'), may hold values from -0.375 to 0.375
- out_weight_b: bfloat16 [2048, 2048], P('tp'), may hold values from -0.25 to 0.25
- residual: bfloat16 [4096, 2048], P(('sp', 'tp')), may hold values from -6 to 6
- norm_gain: float32 [2048], replicated, may hold values from 0.1 to 1.9
- expert_ids: int32 [4096, 2], P('sp'), may hold values from 0 to 31, as said below
- route_weight: float32 [4096, 2], P('sp'), may hold values from 0.1 to 1
- gate_w: bfloat16 [32, 2048, 1024], P('sp', None, 'tp'), may hold values from -0.125 to 0.125
- up_w: bfloat16 [32, 2048, 1024], P('sp', None, 'tp'), may hold values from -0.125 to 0.125
- down_w: bfloat16 [32, 1024, 2048], P('sp', None, 'tp'), may hold values from -0.1875 to 0.1875
Outputs:
- layer_out: bfloat16 [4096, 2048], P('sp', 'tp')
Inputs may be any that keep to these rules, and one draw needn't show every extreme that they name: `expert_ids`: each row names two different experts of one group (expert e is in group e // 8). In every aligned block of 128 rows (one index of sp) no expert is named more than 16 times, and every expert of one group, the same group for all blocks, is named exactly 16 times. `cumlog_a`: along positions the values of each head never increase. `cumlog_b`: along positions the values of each head never increase.
All inputs are finite; a program needn't handle non-finite values.
Results may differ from a plain program's by a relative error of at most 0.017.
Values may be sent and summed in bfloat16 or wider, within the bound.
A program may use at most 64 MiB of HBM per device.

v0:
```python
import jax
import jax.numpy as jnp
from jax import lax
from jax.sharding import PartitionSpec as P

HDA = 64
HDB = 128
GROUPS = 4
TOP = 2


norm_eps = 1e-05


def side_by_side(arrays, axis, dim, along):
    widths = [a.shape[along] for a in arrays]
    both = jnp.concatenate(arrays, axis=along)
    result = lax.all_gather(both, axis, axis=dim, tiled=True)
    return tuple(jnp.split(result, [sum(widths[:k]) for k in range(1, len(widths))], axis=along))


def cut_along(shard, dim, length):
    shape = shard.shape
    pieces = shard.reshape(*shape[:dim], length, shape[dim] // length, *shape[dim + 1 :])
    return jnp.moveaxis(pieces, dim, 0)


def sum_at_owner(shard, axis, dim):
    pieces = cut_along(shard, dim, lax.axis_size(axis))
    arrived = lax.all_to_all(pieces, axis, split_axis=0, concat_axis=0, tiled=True)
    return arrived.astype(jnp.float32).sum(axis=0)


def copy_for_each(shard, axis):
    length = lax.axis_size(axis)
    return lax.all_to_all(
        jnp.broadcast_to(shard[None], (length, *shard.shape)), axis, 0, 0, tiled=True
    )


def joined_along(pieces, dim):
    pieces = jnp.moveaxis(pieces, 0, dim)
    shape = pieces.shape
    return pieces.reshape(*shape[:dim], shape[dim] * shape[dim + 1], *shape[dim + 2 :])


def gather_directly(shard, axis, dim):
    pieces = copy_for_each(shard, axis)
    return joined_along(pieces, dim)


def fold_group(state, queries, keys_piece, values_piece, cum_query, cum_key, visible, head_size):
    best, total, accum = state
    heads = best.shape[0]
    count = keys_piece.shape[1]
    key_grid = keys_piece.reshape(heads, head_size, count)
    value_grid = values_piece.reshape(heads, head_size, count)
    scores = jnp.einsum(
        "hdq,hdk->hqk", queries, key_grid, preferred_element_type=jnp.float32
    ) * head_size ** (-0.5)
    scores = scores + cum_query[:, :, None] - cum_key[:, None, :]
    scores = jnp.where(visible, scores, -jnp.inf)
    best_new = jnp.max(scores, axis=-1)
    shift = jnp.where(best_new > -jnp.inf, best_new, 0.0)
    keep_old = jnp.exp(best - shift)
    weights = jnp.exp(scores - shift[:, :, None])
    total_new = total * keep_old + jnp.sum(weights, axis=-1)
    added = jnp.einsum(
        "hqk,hdk->hdq", weights.astype(jnp.bfloat16), value_grid, preferred_element_type=jnp.float32
    )
    return (best_new, total_new, accum * keep_old[:, None, :] + added)


def empty_state(heads, head_size, length):
    return (
        jnp.full((heads, length), -jnp.inf, jnp.float32),
        jnp.zeros((heads, length), jnp.float32),
        jnp.zeros((heads, head_size, length), jnp.float32),
    )


def finish_state(state):
    accum = state[2] / state[1][:, None, :]
    return accum.astype(jnp.bfloat16).reshape(-1, accum.shape[2])


def per_device(
    query_a,
    key_a,
    value_a,
    cumlog_a,
    query_b,
    key_b,
    value_b,
    cumlog_b,
    out_weight_a,
    out_weight_b,
    residual,
    norm_gain,
    expert_ids,
    route_weight,
    gate_w,
    up_w,
    down_w,
):
    local_tokens = query_a.shape[1]
    heads_a = cumlog_a.shape[0]
    heads_b = cumlog_b.shape[0]
    my_start = lax.axis_index("sp") * local_tokens
    last_query = my_start + local_tokens - 1
    query_pos = my_start + jnp.arange(local_tokens, dtype=jnp.int32)
    cum_query_a = lax.dynamic_slice_in_dim(cumlog_a, my_start, local_tokens, 1)
    cum_query_b = lax.dynamic_slice_in_dim(cumlog_b, my_start, local_tokens, 1)
    grid_a = query_a.reshape(heads_a, HDA, local_tokens)
    grid_b = query_b.reshape(heads_b, HDB, local_tokens)
    keys_a, vals_a, keys_b, vals_b = side_by_side((key_a, value_a, key_b, value_b), "sp", 1, 0)
    count = keys_a.shape[1]

    def visit(state):
        key_pos = jnp.arange(count, dtype=jnp.int32)
        visible = key_pos[None, None, :] <= query_pos[None, :, None]
        new_a = fold_group(state[0], grid_a, keys_a, vals_a, cum_query_a, cumlog_a, visible, HDA)
        new_b = fold_group(state[1], grid_b, keys_b, vals_b, cum_query_b, cumlog_b, visible, HDB)
        return (new_a, new_b)

    def leave(state):
        return state

    state_a, state_b = lax.cond(
        jnp.int32(0) <= last_query,
        visit,
        leave,
        (empty_state(heads_a, HDA, local_tokens), empty_state(heads_b, HDB, local_tokens)),
    )
    attn_a = finish_state(state_a)
    attn_b = finish_state(state_b)
    term = lax.dot_general(
        attn_a, out_weight_a, (((0,), (0,)), ((), ())), preferred_element_type=jnp.float32
    )
    mixed = sum_at_owner(
        (
            term
            + lax.dot_general(
                attn_b, out_weight_b, (((0,), (0,)), ((), ())), preferred_element_type=jnp.float32
            )
        ).astype(jnp.bfloat16),
        "tp",
        0,
    )
    summed = residual.astype(jnp.float32) + mixed
    center = summed - jnp.mean(summed, axis=-1, keepdims=True)
    variance = jnp.mean(center * center, axis=-1, keepdims=True)
    normed = (center * lax.rsqrt(variance + norm_eps) * norm_gain).astype(jnp.bfloat16)
    normed_all = gather_directly(normed, "tp", 0)
    experts = lax.axis_size("sp")
    group_size = experts // GROUPS
    capacity = local_tokens // group_size
    features = normed_all.shape[1]
    flat_ids = expert_ids.reshape(-1)
    marks = (flat_ids[:, None] == jnp.arange(experts, dtype=jnp.int32)[None, :]).astype(jnp.int32)
    rank = jnp.sum((jnp.cumsum(marks, axis=0) - marks) * marks, axis=1)
    slot = flat_ids * capacity + rank
    token_of = jnp.arange(local_tokens * TOP, dtype=jnp.int32) // TOP
    table = jnp.zeros((experts * capacity,), jnp.int32).at[slot].set(token_of)
    filled = jnp.zeros((experts * capacity,), jnp.bfloat16).at[slot].set(1.0)
    send = (normed_all[table] * filled[:, None]).reshape(experts, capacity, features)
    share = capacity // lax.axis_size("tp")
    own_slots = lax.dynamic_slice_in_dim(send, lax.axis_index("tp") * share, share, 1)
    arrived = lax.all_to_all(own_slots, "sp", split_axis=0, concat_axis=0, tiled=True)
    rows = gather_directly(arrived, "tp", 1)
    sources, items, row_width = rows.shape
    flat_rows = rows.reshape(sources * items, row_width)
    gate = jnp.dot(flat_rows, gate_w[0], preferred_element_type=jnp.float32)
    upper = jnp.dot(flat_rows, up_w[0], preferred_element_type=jnp.float32)
    hidden = (jax.nn.silu(gate) * upper).astype(jnp.bfloat16).reshape(sources, items, -1)
    hidden_all = gather_directly(hidden, "tp", 2)
    result = jnp.dot(
        hidden_all.reshape(sources * items, -1), down_w[0], preferred_element_type=jnp.float32
    )
    result = result.astype(jnp.bfloat16).reshape(sources, items, -1)
    returned = lax.all_to_all(result, "sp", split_axis=0, concat_axis=0, tiled=True)
    flat_back = returned.reshape(experts * capacity, -1)
    picked = flat_back[slot].reshape(local_tokens, TOP, -1).astype(jnp.float32)
    routed = jnp.sum(picked * route_weight[:, :, None], axis=1)
    columns = routed.shape[1]
    own_cols = lax.dynamic_slice_in_dim(normed_all, lax.axis_index("tp") * columns, columns, 1)
    return (own_cols.astype(jnp.float32) + routed).astype(jnp.bfloat16)


def solution(mesh):
    placed = (
        P("tp", "sp"),
        P("tp", "sp"),
        P("tp", "sp"),
        P("tp", None),
        P("tp", "sp"),
        P("tp", "sp"),
        P("tp", "sp"),
        P("tp", None),
        P("tp", None),
        P("tp", None),
        P(("sp", "tp"), None),
        P(),
        P("sp", None),
        P("sp", None),
        P("sp", None, "tp"),
        P("sp", None, "tp"),
        P("sp", None, "tp"),
    )
    return jax.shard_map(
        per_device, mesh=mesh, in_specs=placed, out_specs=P("sp", "tp"), check_vma=False
    )
```

profile of v0, /device:TPU:1, one launch (start us, length us, event | category | flops | bytes accessed | tf_op | source)
XLA Modules:
  0.0 261.7 jit_solution(16198794032110819817)
XLA Ops:
  6.5 1.5 pad_maximum_fusion
  8.0 0.8 copy.33
  9.0 0.1 eq.25
  9.1 0.6 reduce-window.6
  9.7 0.2 slice_reduce_fusion
  9.9 81.4 %all-gather.2.cloned.1.call-done = bf16[384,4096]{1,0:T(8,128)(2,1)} async-done(((bf16[384,128]{1,0:T(8,128)(2,1)}), bf16[384,4096]{1,0:T(8,128)(2,1)}) %all-gather.2.cloned.1.call-update) | async-done | bytes 3145744 | tf_op jit(solution)/shard_map/all_gather | solution.py:18
  91.4 6.0 %conditional.1 = (f32[1,128]{1,0:T(1,128)S(1)}, f32[1,64,128]{2,1,0:T(8,128)S(1)}, f32[1,128]{1,0:T(1,128)S(1)}, f32[1,128,128]{1,2,0:T(8,128)S(1)}) conditional(s32[]{:T(128)} %convert_element_type.61, () %tuple.20, (s32[]{:T(128)}, s32[128]{0:T(128)S(1)}, bf16[384,4096]{1,0:T(8,128)(2,1)}, bf16[64,128]{1,0:T(8,128)(2,1)}, f32[1,4096]{1,0:T(1,128)}, ...), branch_computations={%region_0.0_spmd, %region_1.6_spmd} | conditional | flops 413165440 | bytes 28639390 | solution.py:129
  91.4 0.9 dynamic-slice_bitcast_fusion
  92.3 2.1 fusion.49
  94.5 0.6 fusion.10
  95.1 0.4 fusion.9
  95.6 0.8 fusion.48
  96.4 0.6 fusion.11
  97.0 0.4 fusion.7
  97.4 0.3 fusion.42
  97.8 1.1 fusion.29
  98.9 6.5 %all-to-all-start = ((bf16[16,8,2048]{2,1,0:T(8,128)(2,1)}), bf16[16,8,2048]{2,1,0:T(8,128)(2,1)S(1)}, u32[]{:S(2)}, u32[]{:S(2)}) async-start(bf16[16,8,2048]{2,1,0:T(8,128)(2,1)} %fusion.29), calls=%async_computation | async-start | bytes 1048576 | tf_op jit(solution)/shard_map/all_to_all | solution.py:30
  105.6 0.1 mul.103
  105.9 10.4 %all-to-all-done = bf16[16,8,2048]{2,1,0:T(8,128)(2,1)S(1)} async-done(((bf16[16,8,2048]{2,1,0:T(8,128)(2,1)}), bf16[16,8,2048]{2,1,0:T(8,128)(2,1)S(1)}, u32[]{:S(2)}, u32[]{:S(2)}) %all-to-all-start) | async-done | bytes 524320 | tf_op jit(solution)/shard_map/all_to_all | solution.py:30
  116.5 0.2 multiply_reduce_fusion
  116.8 0.8 broadcast_in_dim.46
  117.7 3.6 %all-to-all-start.1 = ((bf16[16,8,2048]{2,1,0:T(8,128)(2,1)}), bf16[16,8,2048]{2,1,0:T(8,128)(2,1)S(1)}, u32[]{:S(2)}, u32[]{:S(2)}) async-start(bf16[16,8,2048]{2,1,0:T(8,128)(2,1)} %broadcast_in_dim.46), calls=%async_computation.1 | async-start | bytes 1048576 | tf_op jit(solution)/shard_map/all_to_all | solution.py:36
  121.3 1.4 scatter_custom_fusion
  122.7 2.2 scatter_custom_fusion.1
  125.0 6.3 %all-to-all-done.1 = bf16[16,8,2048]{2,1,0:T(8,128)(2,1)S(1)} async-done(((bf16[16,8,2048]{2,1,0:T(8,128)(2,1)}), bf16[16,8,2048]{2,1,0:T(8,128)(2,1)S(1)}, u32[]{:S(2)}, u32[]{:S(2)}) %all-to-all-start.1) | async-done | bytes 524320 | tf_op jit(solution)/shard_map/all_to_all | solution.py:36
  131.3 2.5 gather_fusion
  133.8 0.4 dynamic-slice_multiply_fusion
  134.2 0.5 broadcast.364
  134.7 1.4 reduce.22
  136.1 25.1 %all_to_all.30 = bf16[32,2,1024]{2,1,0:T(2,128)(2,1)S(1)} all-to-all(bf16[32,2,1024]{2,1,0:T(2,128)(2,1)S(1)} %reshape.359), channel_id=1, replica_groups=mesh['sp'=32,'tp'=16] {'sp'}, dimensions={0} | all-to-all | bytes 262144 | tf_op jit(solution)/shard_map/all_to_all | solution.py:169
  161.5 0.2 broadcast_in_dim.51
  161.7 29.5 %all_to_all.31 = bf16[16,32,1,2048]{3,1,2,0:T(8,128)(2,1)S(1)} all-to-all(bf16[16,32,1,2048]{3,1,2,0:T(8,128)(2,1)S(1)} %broadcast_in_dim.51), channel_id=1, replica_groups=mesh['sp'=32,'tp'=16] {'tp'}, dimensions={0} | all-to-all | bytes 4194304 | tf_op jit(solution)/shard_map/all_to_all | solution.py:36
  191.2 1.2 copy.36
  192.4 0.8 fusion.33
  193.2 0.2 copy-done.11
  193.3 0.8 fusion.30
  194.2 0.4 broadcast_in_dim.53
  194.7 2.3 reshape.361
  196.9 19.0 %all_to_all.32 = bf16[16,2,16384]{2,1,0:T(2,128)(2,1)} all-to-all(bf16[16,2,16384]{2,1,0:T(2,128)(2,1)} %reshape.361), channel_id=1, replica_groups=mesh['sp'=32,'tp'=16] {'tp'}, dimensions={0} | all-to-all | bytes 2097152 | tf_op jit(solution)/shard_map/all_to_all | solution.py:36
  215.9 3.8 %reshape.362 = bf16[16,32,16,64]{3,2,1,0:T(8,128)(2,1)S(1)} reshape(bf16[16,2,16384]{2,1,0:T(2,128)(2,1)} %all_to_all.32) | data formatting | bytes 2097152
  219.7 3.8 %copy.38 = bf16[32,16,16,64]{3,2,1,0:T(8,128)(2,1)} copy(bf16[32,16,16,64]{3,1,0,2:T(8,128)(2,1)S(1)} %bitcast.89) | data formatting | bytes 2097152 | tf_op jit(solution)/shard_map/transpose | solution.py:42
  223.5 3.3 %reshape_reshape.7 = bf16[512,1024]{1,0:T(8,128)(2,1)S(1)} reshape(bf16[32,16,16,64]{3,2,1,0:T(8,128)(2,1)} %copy.38) | data formatting | bytes 2097152 | tf_op jit(solution)/shard_map/reshape;reshape | solution.py:178
  226.8 1.1 convolution_convert_fusion
  227.9 9.4 %all-to-all-start.5 = ((bf16[32,16,128]{2,1,0:T(8,128)(2,1)}), bf16[32,16,128]{2,1,0:T(8,128)(2,1)S(1)}, u32[]{:S(2)}, u32[]{:S(2)}) async-start(bf16[32,16,128]{2,1,0:T(8,128)(2,1)} %bitcast.30), calls=%async_computation.5 | async-start | bytes 262144 | tf_op jit(solution)/shard_map/all_to_all | solution.py:181
  237.4 15.7 %all-to-all-done.5 = bf16[32,16,128]{2,1,0:T(8,128)(2,1)S(1)} async-done(((bf16[32,16,128]{2,1,0:T(8,128)(2,1)}), bf16[32,16,128]{2,1,0:T(8,128)(2,1)S(1)}, u32[]{:S(2)}, u32[]{:S(2)}) %all-to-all-start.5) | async-done | bytes 131104 | tf_op jit(solution)/shard_map/all_to_all | solution.py:181
  253.2 0.9 gather_fusion.1
  254.0 0.2 fusion.35
  254.3 0.6 add_convert_fusion
  (59 shorter events, 1.5 us)
Async XLA Ops:
  6.5 91.3 %copy-start = (bf16[128,2048]{1,0:T(8,128)(2,1)S(1)}, bf16[128,2048]{1,0:T(8,128)(2,1)}, u32[]{:S(2)}) copy-start(bf16[128,2048]{1,0:T(8,128)(2,1)} %param.28) | copy-start | bytes 1572868
  6.5 84.9 %all-gather.2.cloned.1.call-start = ((), (), s32[]{:S(2)}) async-start(), calls=%async_computation.6 | async-start | bytes 3244032 | tf_op jit(solution)/shard_map/all_gather | solution.py:18
  9.9 81.5 %copy-start.7 = (s32[32,3]{0,1:T(4,128)}, s32[32,3]{0,1:T(4,128)S(1)}, u32[]{:S(2)}) copy-start(s32[32,3]{0,1:T(4,128)S(1)} %reduce-window.9) | copy-start | bytes 1156
  91.4 6.0 %copy-start.3 = (bf16[64,2048]{1,0:T(8,128)(2,1)S(1)}, bf16[64,2048]{1,0:T(8,128)(2,1)}, u32[]{:S(2)}) copy-start(bf16[64,2048]{1,0:T(8,128)(2,1)} %param.27) | copy-start | bytes 786436
  91.4 3.1 %copy-start.1 = (bf16[384,4096]{1,0:T(8,128)(2,1)S(1)}, bf16[384,4096]{1,0:T(8,128)(2,1)}, u32[]{:S(2)}) copy-start(bf16[384,4096]{1,0:T(8,128)(2,1)} %get-tuple-element.135) | copy-start | bytes 9437188 | tf_op jit(solution)/shard_map/cond
  94.5 1.1 copy-start.10
  94.5 1.1 copy-start.12
  97.4 8.1 %copy-start.8 = (s32[128,2]{0,1:T(2,128)S(1)}, s32[128,2]{0,1:T(2,128)}, u32[]{:S(2)}) copy-start(s32[128,2]{0,1:T(2,128)} %param.31) | copy-start | bytes 3076
  97.4 8.3 %slice-start = ((s32[32,3]{0,1:T(4,128)}), s32[32,2]{0,1:T(2,128)S(1)}, s32[]{:S(2)}) async-start(s32[32,3]{0,1:T(4,128)} %copy-done.7), calls=%async_computation.7 | async-start | bytes 2048 | tf_op jit(solution)/shard_map/slice.1
  97.8 18.6 %copy-start.2 = (bf16[8,2048]{1,0:T(8,128)(2,1)S(1)}, bf16[8,2048]{1,0:T(8,128)(2,1)}, u32[]{:S(2)}) copy-start(bf16[8,2048]{1,0:T(8,128)(2,1)} %param.29) | copy-start | bytes 98308
  97.8 19.0 %copy-start.6 = (f32[2048]{0:T(1024)S(1)}, f32[2048]{0:T(1024)}, u32[]{:S(2)}) copy-start(f32[2048]{0:T(1024)} %param.30) | copy-start | bytes 24580
  98.9 17.4 %all-to-all-start = ((bf16[16,8,2048]{2,1,0:T(8,128)(2,1)}), bf16[16,8,2048]{2,1,0:T(8,128)(2,1)S(1)}, u32[]{:S(2)}, u32[]{:S(2)}) async-start(bf16[16,8,2048]{2,1,0:T(8,128)(2,1)} %fusion.29), calls=%async_computation | async-start | bytes 1048576 | tf_op jit(solution)/shard_map/all_to_all | solution.py:30
  117.7 13.7 %all-to-all-start.1 = ((bf16[16,8,2048]{2,1,0:T(8,128)(2,1)}), bf16[16,8,2048]{2,1,0:T(8,128)(2,1)S(1)}, u32[]{:S(2)}, u32[]{:S(2)}) async-start(bf16[16,8,2048]{2,1,0:T(8,128)(2,1)} %broadcast_in_dim.46), calls=%async_computation.1 | async-start | bytes 1048576 | tf_op jit(solution)/shard_map/all_to_all | solution.py:36
  191.2 1.2 copy-start.4
  192.4 1.0 copy-start.11
  223.5 3.3 %copy-start.5 = (bf16[1,1024,128]{2,1,0:T(8,128)(2,1)S(1)}, bf16[1,1024,128]{2,1,0:T(8,128)(2,1)}, u32[]{:S(2)}) copy-start(bf16[1,1024,128]{2,1,0:T(8,128)(2,1)} %param.35) | copy-start | bytes 786436
  223.5 13.8 %copy-start.9 = (f32[128,2]{0,1:T(2,128)S(1)}, f32[128,2]{0,1:T(2,128)}, u32[]{:S(2)}) copy-start(f32[128,2]{0,1:T(2,128)} %param.32) | copy-start | bytes 3076
  227.9 25.3 %all-to-all-start.5 = ((bf16[32,16,128]{2,1,0:T(8,128)(2,1)}), bf16[32,16,128]{2,1,0:T(8,128)(2,1)S(1)}, u32[]{:S(2)}, u32[]{:S(2)}) async-start(bf16[32,16,128]{2,1,0:T(8,128)(2,1)} %bitcast.30), calls=%async_computation.5 | async-start | bytes 262144 | tf_op jit(solution)/shard_map/all_to_all | solution.py:181
Sparse Core Ops, SparseCore 0:
  9.4 81.9 all-gather.1
where the time goes:
time: 262 us
  waiting for transfers between devices  114 us (44%)
  blocking collectives  73.7 us (28%)
  local copies, waits for them, and re-layouts  26.4 us (10%)
  starting transfers between devices  19.5 us (7%)
  between operations  13.7 us (5%)
  matrix products  8.12 us (3%)
  other arithmetic  6.28 us (2%)
    all_gather x1, waiting for transfers between devices, side_by_side(): result = lax.all_gather(both, axis, axis=dim, tiled=True)  81.4 us
    all_to_all x2, blocking collectives, copy_for_each(): lax.all_to_all(jnp.broadcast_to(shard[None], (length, *shard.shape)), axi...  48.5 us
    all_to_all x1, blocking collectives, per_device(): lax.all_to_all(own_slots, 'sp', split_axis=0, concat_axis=0, tiled=True)  25.1 us
    all_to_all x1, waiting for transfers between devices, per_device(): lax.all_to_all(result, 'sp', split_axis=0, concat_axis=0, tiled=True)  15.7 us
    all_to_all x1, waiting for transfers between devices, sum_at_owner(): lax.all_to_all(pieces, axis, split_axis=0, concat_axis=0, tiled=True)  10.4 us
    all_to_all x1, starting transfers between devices, per_device(): lax.all_to_all(result, 'sp', split_axis=0, concat_axis=0, tiled=True)  9.44 us
    unnamed x27, local copies, waits for them, and re-layouts  7.41 us
    all_to_all x1, starting transfers between devices, sum_at_owner(): lax.all_to_all(pieces, axis, split_axis=0, concat_axis=0, tiled=True)  6.53 us
  transfers between devices with their start and end apart: 4, of which 4 were waited for; matrix products, arithmetic and copies ran while one was open for 2% of the time, Pallas kernels for 0%

commit v1 on v0

v1 whole, which is shorter than its diff:
```python
import jax
import jax.numpy as jnp
from jax import lax
from jax.experimental import pallas as pl
from jax.experimental.pallas import tpu as pltpu
from jax.sharding import PartitionSpec as P

MESH = pl.DeviceIdType.MESH
F32 = jnp.float32
BF16 = jnp.bfloat16
HDA = 64
HDB = 128
NZ = 16
HALF = NZ // 2
LOG2E = 1.4426950408889634
NORM_EPS = 1e-05


def remote(src, dst, send_sem, recv_sem, device):
    return pltpu.make_async_remote_copy(
        src_ref=src, dst_ref=dst, send_sem=send_sem, recv_sem=recv_sem,
        device_id=device, device_id_type=MESH,
    )


def nt(a, b):
    return lax.dot_general(a, b, (((1,), (1,)), ((), ())), preferred_element_type=F32)


def nn(a, b):
    return lax.dot_general(a, b, (((1,), (0,)), ((), ())), preferred_element_type=F32)


def kernel(
    qa_ref, ka_ref, va_ref, cuma_ref, qb_ref, kb_ref, vb_ref, cumb_ref,
    woa_ref, wob_ref, res_ref, gain_ref, ids_ref, rw_ref, gate_ref, up_ref, down_ref,
    out_ref,
    kv, wall, dall, woa, wob, qta, qtb, top_a, top_b, sum_a, sum_b, acc_a, acc_b,
    pick, mix_hi, mix_lo, rs_send, rs_recv, n_send, n_recv, d_send, xr, xall,
    h_own, hall, o_send, ret,
    load_sem, kv_recv_p, kv_recv_m, kv_recv_s, kv_send_p, kv_send_m, kv_send_s,
    w_recv, w_send, rs_sems, n_sems, d_sems, x_recv, x_send, h_recv, h_send, o_sems,
):
    sp = lax.axis_index("sp")
    tp = lax.axis_index("tp")
    z, c = sp // 2, sp % 2
    y, x = tp // 4, tp % 4
    quarter = z % 4
    place = (z // 4) * 2 + c
    at_home = y == quarter
    up_z = (2 * ((z + 1) % NZ) + c, tp)
    down_z = (2 * ((z + NZ - 1) % NZ) + c, tp)
    sibling = (2 * z + 1 - c, tp)
    up_y = (sp, ((y + 1) % 4) * 4 + x)
    down_y = (sp, ((y + 3) % 4) * 4 + x)

    barrier = pltpu.get_barrier_semaphore()
    for device in (up_z, down_z, sibling):
        pl.semaphore_signal(barrier, inc=1, device_id=device, device_id_type=MESH)

    @pl.loop(1, 16)
    def _(r):
        pl.semaphore_signal(barrier, inc=1, device_id=(sp, (tp + r) % 16), device_id_type=MESH)

    @pl.loop(0, 32)
    def _(e):
        @pl.when(jnp.logical_or(e != sp, jnp.logical_not(at_home)))
        def _():
            pl.semaphore_signal(barrier, inc=1, device_id=(e, quarter * 4 + x), device_id_type=MESH)

        i, ys = e % 8, e // 8
        s = 2 * (y + 4 * (i // 2)) + i % 2

        @pl.when(jnp.logical_or(s != sp, ys != y))
        def _():
            pl.semaphore_signal(barrier, inc=1, device_id=(s, ys * 4 + x), device_id_type=MESH)

    own = kv.at[sp]
    kv_loads = [
        pltpu.make_async_copy(ka_ref, own.at[0, pl.ds(0, HDA)], load_sem.at[0]),
        pltpu.make_async_copy(va_ref, own.at[0, pl.ds(HDA, HDA)], load_sem.at[1]),
        pltpu.make_async_copy(kb_ref, own.at[1], load_sem.at[2]),
        pltpu.make_async_copy(vb_ref, own.at[2], load_sem.at[3]),
    ]
    w_loads = [
        pltpu.make_async_copy(gate_ref, wall.at[y, pl.ds(0, 64)], load_sem.at[4]),
        pltpu.make_async_copy(up_ref, wall.at[y, pl.ds(64, 64)], load_sem.at[5]),
    ]
    o_loads = [
        pltpu.make_async_copy(woa_ref, woa, load_sem.at[6]),
        pltpu.make_async_copy(wob_ref, wob, load_sem.at[7]),
    ]
    d_loads = [
        pltpu.make_async_copy(
            down_ref.at[pl.ds((4 * b + a) * 64, 64)],
            dall.at[y, pl.ds((4 * a + b) * 64, 64)],
            load_sem.at[8 + 4 * a + b],
        )
        for a in range(4)
        for b in range(4)
    ]
    for copy in kv_loads + w_loads + d_loads + o_loads:
        copy.start()

    expert_of = lax.broadcasted_iota(jnp.int32, (32, 128), 0)
    id0, id1 = ids_ref[0:1, :], ids_ref[1:2, :]
    marks = (expert_of == id0).astype(F32) + (expert_of == id1).astype(F32)
    before = lax.broadcasted_iota(jnp.int32, (128, 128), 0) < lax.broadcasted_iota(
        jnp.int32, (128, 128), 1
    )
    rank = nn(marks.astype(BF16), before.astype(F32).astype(BF16))
    spread = (
        lax.broadcasted_iota(jnp.int32, (512, 32), 0) // 16
        == lax.broadcasted_iota(jnp.int32, (512, 32), 1)
    ).astype(F32).astype(BF16)
    marks_at = nn(spread, marks.astype(BF16))
    rank_at = nn(spread, rank.astype(BF16))
    slot = lax.broadcasted_iota(jnp.int32, (512, 128), 0)
    chosen = jnp.logical_and(marks_at > 0.5, rank_at == (slot % 16).astype(F32))
    pick[...] = chosen.astype(F32).astype(BF16)
    weight = jnp.where(
        chosen, jnp.where(slot // 16 == id0, rw_ref[0:1, :], rw_ref[1:2, :]), 0.0
    )
    weight_t = weight.T
    high = weight_t.astype(BF16)
    mix_hi[...] = high
    mix_lo[...] = (weight_t - high.astype(F32)).astype(BF16)
    qta[...] = qa_ref[...].astype(F32).T.astype(BF16)
    qtb[...] = qb_ref[...].astype(F32).T.astype(BF16)
    for ref in (top_a, top_b):
        ref[...] = jnp.full(ref.shape, -jnp.inf, F32)
    for ref in (sum_a, sum_b, acc_a, acc_b):
        ref[...] = jnp.zeros(ref.shape, F32)

    for copy in kv_loads + w_loads + d_loads:
        copy.wait()
    at_home_count = jnp.where(at_home, 1, 0)
    pl.semaphore_wait(barrier, 18 + 2 * (32 - at_home_count))

    def send_p(k, j):
        src = 2 * (z - k + NZ) % (2 * NZ) + c
        return remote(kv.at[src, j], kv.at[src, j], kv_send_p.at[k, j], kv_recv_p.at[k, j], up_z)

    def recv_p(k, j):
        src = 2 * (z - k) + c
        return remote(
            kv.at[src, j], kv.at[src, j], kv_send_p.at[k, j], kv_recv_p.at[k - 1, j], up_z
        )

    def send_m(k, j):
        src = 2 * ((z + k) % NZ) + c
        return remote(kv.at[src, j], kv.at[src, j], kv_send_m.at[k, j], kv_recv_m.at[k, j], down_z)

    def recv_m(k, j):
        src = 2 * ((z + k) % NZ) + c
        return remote(
            kv.at[src, j], kv.at[src, j], kv_send_m.at[k, j], kv_recv_m.at[k - 1, j], down_z
        )

    def send_s(zz):
        src = 2 * zz + c
        return remote(kv.at[src], kv.at[src], kv_send_s.at[zz], kv_recv_s.at[zz], sibling)

    def recv_s(zz):
        src = 2 * zz + 1 - c
        return remote(kv.at[src], kv.at[src], kv_send_s.at[zz], kv_recv_s.at[zz], sibling)

    def valid_p(k):
        return z - k >= 0

    def go_p(k):
        return jnp.logical_and(z - k >= 0, z < NZ - 1)

    def valid_m(k):
        return (z + k) % NZ <= HALF - 2

    def useful_m(k):
        return z + k - NZ >= 0

    def fold(shards, masked):
        zs = [kv.at[s] for s in shards]
        keys_a = jnp.concatenate([s[0, 0:HDA] for s in zs], axis=1)
        vals_a = jnp.concatenate([s[0, HDA : 2 * HDA] for s in zs], axis=1)
        keys_b = jnp.concatenate([s[1] for s in zs], axis=1)
        vals_b = jnp.concatenate([s[2] for s in zs], axis=1)
        for keys, vals, qt, cum, top, total, acc, size in (
            (keys_a, vals_a, qta, cuma_ref, top_a, sum_a, acc_a, HDA),
            (keys_b, vals_b, qtb, cumb_ref, top_b, sum_b, acc_b, HDB),
        ):
            at = pl.multiple_of(sp * 128, 128)
            base = cum[0:1, pl.ds(at, 128)][0:1, 0:1]
            bias = jnp.concatenate(
                [
                    (base - cum[0:1, pl.ds(pl.multiple_of(s * 128, 128), 128)]) * LOG2E
                    for s in shards
                ],
                axis=1,
            )
            scores = nn(qt[...], keys) * (size**-0.5 * LOG2E) + bias
            if masked:
                hidden = lax.broadcasted_iota(jnp.int32, scores.shape, 1) > (
                    lax.broadcasted_iota(jnp.int32, scores.shape, 0)
                )
                scores = jnp.where(hidden, -jnp.inf, scores)
            old = top[:, 0:1]
            new = jnp.maximum(old, jnp.max(scores, axis=1, keepdims=True))
            keep = jnp.exp2(old - new)
            weights = jnp.exp2(scores - new)
            added = jnp.sum(weights, axis=1, keepdims=True)
            total[...] = total[...] * keep + added
            acc[...] = acc[...] * keep + nt(weights.astype(BF16), vals)
            top[...] = jnp.broadcast_to(new, top.shape)

    for j in range(3):
        @pl.when(z < NZ - 1)
        def _():
            send_p(0, j).start()

        @pl.when(z <= HALF - 2)
        def _():
            send_m(0, j).start()

    @pl.when(c == 0)
    def _():
        send_s(z).start()

    def part(v, half):
        return wall.at[v, pl.ds(64 * half, 64)] if half < 2 else dall.at[v, pl.ds(512 * (half - 2), 512)]

    def w_first(half, sign):
        index = half * 3 + (0 if sign > 0 else 1)
        device = up_y if sign > 0 else down_y
        return remote(part(y, half), part(y, half), w_send.at[index], w_recv.at[index], device)

    def w_got(half, sign):
        index = half * 3 + (0 if sign > 0 else 1)
        v = (y + 3) % 4 if sign > 0 else (y + 1) % 4
        return remote(part(v, half), part(v, half), w_send.at[index], w_recv.at[index], up_y)

    def w_relay(half):
        index = half * 3 + 2
        v, device = ((y + 3) % 4, up_y) if half % 2 == 0 else ((y + 1) % 4, down_y)
        return remote(part(v, half), part(v, half), w_send.at[index], w_recv.at[index], device)

    def w_got_relay(half):
        index = half * 3 + 2
        v = (y + 2) % 4
        return remote(part(v, half), part(v, half), w_send.at[index], w_recv.at[index], up_y)

    for half in (0, 1):
        w_first(half, 1 if half == 0 else -1).start()
    for half in (0, 1):
        w_first(half, -1 if half == 0 else 1).start()

    fold([sp], True)

    @pl.when(c == 1)
    def _():
        recv_s(z).wait_recv()
        fold([sp - 1], False)

    def use(zz):
        recv_s(zz).wait_recv()
        fold([2 * zz, 2 * zz + 1], False)

    @pl.loop(1, HALF + 1)
    def _(k):
        for j in range(3):
            @pl.when(valid_p(k))
            def _():
                recv_p(k, j).wait_recv()

            @pl.when(jnp.logical_and(go_p(k), k < HALF))
            def _():
                send_p(k, j).start()

            @pl.when(jnp.logical_and(valid_m(k), k < HALF))
            def _():
                recv_m(k, j).wait_recv()

            @pl.when(jnp.logical_and(valid_m(k), k < HALF - 1))
            def _():
                send_m(k, j).start()

        @pl.when(valid_p(k))
        def _():
            send_s(z - k).start()

        @pl.when(jnp.logical_and(useful_m(k), k < HALF))
        def _():
            send_s(z + k - NZ).start()

        @pl.when(jnp.logical_and(valid_p(k - 1), k > 1))
        def _():
            use(z - k + 1)

        @pl.when(jnp.logical_and(useful_m(k - 1), k > 1))
        def _():
            use(z + k - 1 - NZ)

        @pl.when(k == 4)
        def _():
            w_got(0, 1).wait_recv()
            w_relay(0).start()
            w_got(1, -1).wait_recv()
            w_relay(1).start()
            w_first(2, 1).start()
            w_first(3, -1).start()
            w_first(2, -1).start()
            w_first(3, 1).start()

    @pl.when(valid_p(HALF))
    def _():
        use(z - HALF)

    for copy in o_loads:
        copy.wait()
    attn_a = (acc_a[...] / sum_a[...]).astype(BF16)
    attn_b = (acc_b[...] / sum_b[...]).astype(BF16)
    for n in range(4):
        cols = pl.ds(512 * n, 512)
        term = nn(attn_a, woa[:, cols]) + nn(attn_b, wob[:, cols])
        rs_send[:, :, cols] = term.reshape(16, 8, 512).astype(BF16)

    @pl.loop(1, 16)
    def _(r):
        p = (tp + r) % 16
        remote(rs_send.at[p], rs_recv.at[r - 1], rs_sems.at[0], rs_sems.at[1], (sp, p)).start()

    mixed = rs_send[tp].astype(F32)
    remote(rs_recv, rs_recv, rs_sems.at[0], rs_sems.at[1], up_y).wait_recv()
    for r in range(15):
        mixed = mixed + rs_recv[r].astype(F32)
    summed = res_ref[...].astype(F32) + mixed
    center = summed - jnp.mean(summed, axis=1, keepdims=True)
    variance = jnp.mean(center * center, axis=1, keepdims=True)
    normed_rows = (center * lax.rsqrt(variance + NORM_EPS) * gain_ref[...]).astype(BF16).astype(F32)
    for j in range(16):
        n_send[j] = normed_rows[:, 128 * j : 128 * (j + 1)]
    n_recv[tp] = n_send[tp]

    @pl.loop(1, 16)
    def _(r):
        p = (tp + r) % 16
        remote(n_send.at[p], n_recv.at[tp], n_sems.at[0], n_sems.at[1], (sp, p)).start()

    most = pl.ds(0, 15)
    remote(n_send.at[most], n_recv.at[most], n_sems.at[0], n_sems.at[1], up_y).wait_recv()
    normed = n_recv[...].reshape(128, 128)

    d_send[...] = nn(pick[...], normed.astype(BF16)).astype(BF16).reshape(32, 16, 128)

    @pl.loop(0, 32)
    def _(e):
        @pl.when(jnp.logical_or(e != sp, jnp.logical_not(at_home)))
        def _():
            remote(
                d_send.at[e], xr.at[y * 8 + place], d_sems.at[0], d_sems.at[1],
                (e, quarter * 4 + x),
            ).start()

    w_got(2, 1).wait_recv()
    w_relay(2).start()
    w_got(3, -1).wait_recv()
    w_relay(3).start()

    @pl.when(at_home)
    def _():
        xr[y * 8 + place] = d_send[sp]

    def wait_32(ref, sems):
        for count, flag in ((31, at_home), (32, jnp.logical_not(at_home))):
            @pl.when(flag)
            def _():
                view = ref.at[pl.ds(0, count)]
                remote(view, view, sems.at[0], sems.at[1], up_y).wait_recv()

    wait_32(xr, d_sems)
    for r in range(1, 4):
        remote(
            xr, xall.at[r - 1], x_send.at[r - 1], x_recv.at[r - 1], (sp, y * 4 + (x + r) % 4)
        ).start()

    w_got(0, -1).wait_recv()
    w_got(1, 1).wait_recv()
    w_got_relay(0).wait_recv()
    w_got_relay(1).wait_recv()

    def gate_up(ref, xx):
        lhs, gates, ups = [], [], []
        for ys in range(4):
            lhs.append(ref[8 * ys : 8 * ys + 8].reshape(128, 128))
            cols = pl.ds(pl.multiple_of((4 * ys + xx) * 128, 128), 128)
            gates.append(wall[:, 0:64, cols].reshape(256, 128))
            ups.append(wall[:, 64:128, cols].reshape(256, 128))
        lhs = jnp.concatenate(lhs, axis=1)
        return nt(lhs, jnp.concatenate(gates, axis=1)), nt(lhs, jnp.concatenate(ups, axis=1))

    gate, upper = gate_up(xr, x)
    for r in (1, 3, 2):
        remote(
            xr, xall.at[r - 1], x_send.at[r - 1], x_recv.at[r - 1], up_y
        ).wait_recv()
        more_gate, more_up = gate_up(xall.at[r - 1], (x + 4 - r) % 4)
        gate, upper = gate + more_gate, upper + more_up
    h_own[...] = (gate / (1.0 + jnp.exp(-gate)) * upper).astype(BF16)
    for r in range(1, 4):
        remote(
            h_own, hall.at[r - 1], h_send.at[r - 1], h_recv.at[r - 1], (sp, y * 4 + (x + r) % 4)
        ).start()

    w_got(2, -1).wait_recv()
    w_got(3, 1).wait_recv()
    w_got_relay(2).wait_recv()
    w_got_relay(3).wait_recv()

    def downward(hidden, xx):
        rows = pl.ds(pl.multiple_of(xx * 256, 256), 256)
        return nn(hidden, jnp.concatenate([dall[v, rows, :] for v in range(4)], axis=1))

    result = downward(h_own[...], x)
    for r in (1, 3, 2):
        remote(
            h_own, hall.at[r - 1], h_send.at[r - 1], h_recv.at[r - 1], up_y
        ).wait_recv()
        result = result + downward(hall[r - 1], (x + 4 - r) % 4)
    for v in range(4):
        o_send[8 * v : 8 * v + 8] = (
            result[:, 128 * v : 128 * (v + 1)].astype(BF16).reshape(8, 16, 128)
        )

    @pl.loop(0, 32)
    def _(n):
        i, v = n % 8, n // 8
        s = 2 * (y + 4 * (i // 2)) + i % 2

        @pl.when(jnp.logical_or(s != sp, v != y))
        def _():
            remote(
                o_send.at[n], ret.at[sp], o_sems.at[0], o_sems.at[1], (s, v * 4 + x)
            ).start()

    @pl.when(at_home)
    def _():
        ret[sp] = o_send[y * 8 + place]

    wait_32(ret, o_sems)
    back = ret[...].reshape(512, 128)
    routed = nn(mix_hi[...], back) + nn(mix_lo[...], back)
    out_ref[...] = (normed + routed).astype(BF16)

    for j in range(3):
        @pl.when(z < NZ - 1)
        def _():
            send_p(0, j).wait_send()

        @pl.when(z <= HALF - 2)
        def _():
            send_m(0, j).wait_send()

    @pl.when(c == 0)
    def _():
        send_s(z).wait_send()

    @pl.loop(1, HALF + 1)
    def _(k):
        for j in range(3):
            @pl.when(jnp.logical_and(go_p(k), k < HALF))
            def _():
                send_p(k, j).wait_send()

            @pl.when(jnp.logical_and(valid_m(k), k < HALF - 1))
            def _():
                send_m(k, j).wait_send()

        @pl.when(valid_p(k))
        def _():
            send_s(z - k).wait_send()

        @pl.when(jnp.logical_and(useful_m(k), k < HALF))
        def _():
            send_s(z + k - NZ).wait_send()

    for half in range(4):
        w_first(half, 1).wait_send()
        w_first(half, -1).wait_send()
        w_relay(half).wait_send()
    remote(rs_recv, rs_recv, rs_sems.at[0], rs_sems.at[1], up_y).wait_send()
    remote(n_send.at[most], n_recv.at[most], n_sems.at[0], n_sems.at[1], up_y).wait_send()
    for r in range(1, 4):
        remote(xr, xall.at[r - 1], x_send.at[r - 1], x_recv.at[r - 1], up_y).wait_send()
        remote(h_own, hall.at[r - 1], h_send.at[r - 1], h_recv.at[r - 1], up_y).wait_send()
    for ref, sems in ((d_send, d_sems), (o_send, o_sems)):
        for count, flag in ((31, at_home), (32, jnp.logical_not(at_home))):
            @pl.when(flag)
            def _():
                view = ref.at[pl.ds(0, count)]
                remote(view, view, sems.at[0], sems.at[1], up_y).wait_send()


def per_device(
    query_a, key_a, value_a, cumlog_a, query_b, key_b, value_b, cumlog_b,
    out_weight_a, out_weight_b, residual, norm_gain, expert_ids, route_weight,
    gate_w, up_w, down_w,
):
    vm = pl.BlockSpec(memory_space=pltpu.VMEM)
    hbm = pl.BlockSpec(memory_space=pl.ANY)
    dma = pltpu.SemaphoreType.DMA
    return pl.pallas_call(
        kernel,
        out_shape=jax.ShapeDtypeStruct((128, 128), BF16),
        in_specs=[
            vm, hbm, hbm, vm, vm, hbm, hbm, vm, hbm, hbm, vm, vm, vm, vm, hbm, hbm, hbm,
        ],
        out_specs=vm,
        scratch_shapes=[
            pltpu.VMEM((32, 3, 128, 128), BF16),
            pltpu.VMEM((4, 128, 2048), BF16),
            pltpu.VMEM((4, 1024, 128), BF16),
            pltpu.VMEM((64, 2048), BF16),
            pltpu.VMEM((128, 2048), BF16),
            pltpu.VMEM((128, 64), BF16),
            pltpu.VMEM((128, 128), BF16),
            pltpu.VMEM((128, 128), F32),
            pltpu.VMEM((128, 128), F32),
            pltpu.VMEM((128, 64), F32),
            pltpu.VMEM((128, 128), F32),
            pltpu.VMEM((128, 64), F32),
            pltpu.VMEM((128, 128), F32),
            pltpu.VMEM((512, 128), BF16),
            pltpu.VMEM((128, 512), BF16),
            pltpu.VMEM((128, 512), BF16),
            pltpu.VMEM((16, 8, 2048), BF16),
            pltpu.VMEM((15, 8, 2048), BF16),
            pltpu.VMEM((16, 8, 128), F32),
            pltpu.VMEM((16, 8, 128), F32),
            pltpu.VMEM((32, 16, 128), BF16),
            pltpu.VMEM((32, 16, 128), BF16),
            pltpu.VMEM((3, 32, 16, 128), BF16),
            pltpu.VMEM((128, 256), BF16),
            pltpu.VMEM((3, 128, 256), BF16),
            pltpu.VMEM((32, 16, 128), BF16),
            pltpu.VMEM((32, 16, 128), BF16),
            dma((24,)),
            dma((HALF, 3)),
            dma((HALF, 3)),
            dma((NZ,)),
            dma((HALF, 3)),
            dma((HALF, 3)),
            dma((NZ,)),
            dma((12,)),
            dma((12,)),
            dma((2,)),
            dma((2,)),
            dma((2,)),
            dma((3,)),
            dma((3,)),
            dma((3,)),
            dma((3,)),
            dma((2,)),
        ],
        compiler_params=pltpu.CompilerParams(
            collective_id=0, has_side_effects=True, vmem_limit_bytes=48 * 1024 * 1024
        ),
        name="layer",
    )(
        query_a, key_a, value_a, cumlog_a, query_b, key_b, value_b, cumlog_b,
        out_weight_a, out_weight_b, residual, norm_gain.reshape(1, -1),
        expert_ids.T, route_weight.T, gate_w[0].T, up_w[0].T, down_w[0],
    )


def solution(mesh):
    placed = (
        P("tp", "sp"), P("tp", "sp"), P("tp", "sp"), P("tp", None),
        P("tp", "sp"), P("tp", "sp"), P("tp", "sp"), P("tp", None),
        P("tp", None), P("tp", None), P(("sp", "tp"), None), P(),
        P("sp", None), P("sp", None),
        P("sp", None, "tp"), P("sp", None, "tp"), P("sp", None, "tp"),
    )
    return jax.shard_map(
        per_device, mesh=mesh, in_specs=placed, out_specs=P("sp", "tp"), check_vma=False
    )
```

time: 262 us -> 112 us (0.43)
  the two profiles are of different devices: /device:TPU:1 before, /device:TPU:57 now
where the time goes in v1:
time: 112 us; the launch traced here: 111 us
  Pallas kernels  98.6 us (88%)
  local copies, waits for them, and re-layouts  12.8 us (11%)
    pallas_call x1, Pallas kernels, per_device(): pl.pallas_call(kernel, out_shape=jax.ShapeDtypeStruct((128, 128), BF16),...  98.6 us
    unnamed x35, local copies, waits for them, and re-layouts  12.8 us

profile of v1, /device:TPU:57, one launch (start us, length us, event | category | flops | bytes accessed | tf_op | source)
XLA Modules:
  0.0 111.4 jit_solution(7462113258951432796)
XLA Ops:
  0.0 0.0 copy-start.14
  0.0 0.0 copy-start.16
  0.0 0.0 copy-start.15
  0.0 0.7 copy-done.14
  0.7 0.0 copy-done.16
  0.7 0.0 copy-done.15
  0.7 0.0 copy-start
  0.7 1.0 copy-done
  1.8 0.0 copy-start.1
  1.8 0.9 copy-done.1
  2.7 0.0 copy-start.2
  2.7 0.9 copy-done.2
  3.7 0.0 copy-start.3
  3.7 0.9 copy-done.3
  4.6 0.0 copy-start.4
  4.6 0.9 copy-done.4
  5.6 0.0 copy-start.5
  5.6 0.8 copy-done.5
  6.3 0.0 copy-start.6
  6.3 0.8 copy-done.6
  7.1 0.0 copy-start.7
  7.1 0.8 copy-done.7
  7.8 0.0 copy-start.8
  7.8 0.8 copy-done.8
  8.6 0.0 copy-start.9
  8.6 0.7 copy-done.9
  9.3 0.0 copy-start.10
  9.3 0.7 copy-done.10
  10.0 0.0 copy-start.11
  10.0 0.7 copy-done.11
  10.7 0.0 copy-start.12
  10.7 0.7 copy-done.12
  11.5 0.0 copy-start.13
  11.5 0.7 copy-done.13
  12.2 98.6 %layer.1 = bf16[128,128]{1,0:T(8,128)(2,1)S(1)} custom-call(bf16[64,128]{1,0:T(8,128)(2,1)S(1)} %copy-done.9, bf16[64,128]{1,0:T(8,128)(2,1)S(1)} %copy-done.10, bf16[64,128]{1,0:T(8,128)(2,1)S(1)} %copy-done.11, f32[1,4096]{1,0:T(1,128)S(1)} %copy-done.12, bf16[128,128]{1,0:T(8,128)(2,1)S(1)} %copy-done.5, bf16[128,128]{1,0:T(8,128)(2,1)S(1)} %copy-done.6, ...), custom_call_target="tpu_custom_call" | custom-call | tf_op jit(solution)/shard_map/layer/pallas_call | solution.py:509
  110.8 0.6 copy.19
Async XLA Ops:
  0.0 0.7 copy-start.14
  0.0 0.7 copy-start.16
  0.0 0.7 copy-start.15
  0.7 1.0 copy-start
  1.8 0.9 copy-start.1
  2.7 0.9 copy-start.2
  3.7 0.9 copy-start.3
  4.6 0.9 copy-start.4
  5.6 0.8 copy-start.5
  6.3 0.8 copy-start.6
  7.1 0.8 copy-start.7
  7.8 0.8 copy-start.8
  8.6 0.7 copy-start.9
  9.3 0.7 copy-start.10
  10.0 0.7 copy-start.11
  10.7 0.7 copy-start.12
  11.5 0.7 copy-start.13
